TPU v7x, 32 devices: a whole 2x2x4 slice. The times are simulated.
32 devices in a mesh: fs: 8 (over z, x), tp: 4 (over y, core).
Axes of the slice: x: 2, y: 2, z: 4, core: 2. Of those that a mesh axis runs over, the one named last changes fastest.
Arguments:
- prompts: bfloat16 [4, 1024, 2048], P('tp'), may hold values from -6 to 6
- gain_first: float32 [2048], P('fs'), may hold values from 0.1 to 1.9
- gate_first: float32 [2048, 5632], P('fs', 'tp'), may hold values from -0.125 to 0.125
- up_first: float32 [2048, 5632], P('fs', 'tp'), may hold values from -0.125 to 0.125
- down_first: float32 [5632, 2048], P('fs', 'tp'), may hold values from -0.078125 to 0.078125
- gain_second: float32 [2048], P('fs'), may hold values from 0.1 to 1.9
- gate_second: float32 [2048, 5632], P('fs', 'tp'), may hold values from -0.125 to 0.125
- up_second: float32 [2048, 5632], P('fs', 'tp'), may hold values from -0.125 to 0.125
- down_second: float32 [5632, 2048], P('fs', 'tp'), may hold values from -0.078125 to 0.078125
Outputs:
- served_gate_first: bfloat16 [2048, 5632], P(None, 'fs')
- served_up_first: bfloat16 [2048, 5632], P(None, 'fs')
- served_down_first: bfloat16 [5632, 2048], P('fs')
- served_gate_second: bfloat16 [2048, 5632], P(None, 'fs')
- served_up_second: bfloat16 [2048, 5632], P(None, 'fs')
- served_down_second: bfloat16 [5632, 2048], P('fs')
- prompt_states: bfloat16 [4, 1024, 2048], P('tp', 'fs')
All inputs are finite; a program needn't handle non-finite values.
Results may differ from a plain program's by a relative error of at most 0.012.
Values may be sent and summed in bfloat16 or wider, within the bound.
A program may use at most 128 MiB of HBM per device.

v0:
```python
import functools

import jax
import jax.numpy as jnp
from jax import lax
from jax.experimental import pallas as pl
from jax.experimental.pallas import tpu as pltpu
from jax.sharding import PartitionSpec as P

CORES = 2
CUTS = 2
TILE = 256


def partner(index, step, count):
    if count & (count - 1):
        return (index + step) % count
    result, bit = 0, 1
    while bit < count:
        result = result + ((index // bit + step // bit) % 2) * bit
        bit *= 2
    return result


def tiles(total, size):
    return [(start, min(size, total - start)) for start in range(0, total, size)]


class Ring:
    def __init__(self, n_z, n_x):
        self.n_z, self.n_x, self.n = n_z, n_x, n_z * n_x

    def position(self, z, x):
        if self.n_x == 1:
            return z
        row, wide = self.n_z - 1 - z, self.n_x - 1
        back = self.n_z + row * wide + jnp.where(row % 2 == 0, x - 1, self.n_x - 1 - x)
        return jnp.where(x == 0, z, back)

    def at(self, place):
        place = (place + self.n) % self.n
        if self.n_x == 1:
            return place
        wide = self.n_x - 1
        rest = place + self.n - self.n_z
        row = (rest - self.n) // wide
        col = (rest - self.n) % wide
        back = (self.n_z - 1 - row) * self.n_x + jnp.where(row % 2 == 0, 1 + col, self.n_x - 1 - col)
        return jnp.where(place < self.n_z, place * self.n_x, back)

    def slot(self, offset):
        offset = offset % self.n
        if offset == 0:
            return 0
        if 2 * offset == self.n:
            return 1
        return 2 * offset + 1 if 2 * offset < self.n else 2 * (self.n - offset)


def remote(src, dst, send, recv, f, t):
    return pltpu.make_async_remote_copy(
        src_ref=src, dst_ref=dst, send_sem=send, recv_sem=recv,
        device_id={"fs": f, "tp": t}, device_id_type=pl.DeviceIdType.MESH,
    )


class Exchange:
    def __init__(self, n_fs, n_tp, gu, dn, gu_out, dn_out, sems):
        (self.send_a, self.recv_a, self.send_y, self.recv_y, self.send_m, self.recv_m,
         self.dn_local, self.dn_send_y, self.dn_recv_y, self.dn_send_m, self.dn_recv_m) = sems
        self.n_fs, self.n_tp, self.n_y = n_fs, n_tp, n_tp // CORES
        self.per = n_fs // n_tp
        self.gu, self.dn, self.gu_out, self.dn_out = gu, dn, gu_out, dn_out
        self.hidden, self.rows = gu.shape[1] // self.per, gu.shape[2]
        self.part = self.hidden // self.n_y
        self.me_f, self.me_t = lax.axis_index("fs"), lax.axis_index("tp")
        self.my_y, self.my_c = self.me_t // CORES, self.me_t % CORES
        self.mate = self.my_y * CORES + (1 - self.my_c)
        self.sends = []

    def peer(self, step):
        return (self.my_y + step) % self.n_y

    def window(self, f, y, c):
        return self.gu_out.at[c, pl.ds(pl.multiple_of(y * self.part, 8), self.part),
                              pl.ds(pl.multiple_of(f * self.rows, 128), self.rows)]

    def first(self, i, step):
        q = (self.me_t + step) % self.n_tp
        y, c = q // CORES, q % CORES
        f = self.me_t * self.per + i
        src = self.gu.at[c, pl.ds(pl.multiple_of(i * self.hidden + y * self.part, 8), self.part), :]
        dst = self.window(self.me_f, y, c)
        copy = remote(src, dst, self.send_a.at[i * self.n_tp + step], self.recv_a.at[self.me_f], f, q)
        return copy, src, dst, f == self.me_f

    def start_gu(self):
        for step in range(self.n_tp - 1, -1, -1):
            for i in range(self.per):
                copy, src, dst, here = self.first(i, step)
                if step == 0:
                    @pl.when(here)
                    def _():
                        pltpu.make_async_copy(src, dst, self.recv_a.at[self.me_f]).start()

                    @pl.when(jnp.logical_not(here))
                    def _():
                        copy.start()
                else:
                    copy.start()

    def columns(self, t):
        width = self.dn.shape[1]
        return self.dn_out.at[:, pl.ds(pl.multiple_of(t * width, 128), width)]

    def start_dn(self):
        mine = self.columns(self.me_t)
        self.keep = pltpu.make_async_copy(self.dn, mine, self.dn_local)
        self.keep.start()
        for step in range(1, self.n_y):
            self.sends.append(remote(self.dn, mine, self.dn_send_y.at[step], self.dn_recv_y.at[self.my_y],
                                     self.me_f, self.peer(step) * CORES + self.my_c))
            self.sends[-1].start()
        self.sends.append(remote(self.dn, mine, self.dn_send_m.at[0], self.dn_recv_m.at[self.my_y],
                                 self.me_f, self.mate))
        self.sends[-1].start()

    def pass_first(self):
        for step in range(self.n_fs):
            f = partner(self.me_f, step, self.n_fs)
            piece = self.window(f, self.my_y, self.my_c)
            slot = self.my_y * self.n_fs + f
            remote(piece, piece, self.send_m.at[0], self.recv_a.at[f], self.me_f, self.mate).wait_recv()
            for hop in range(1, self.n_y):
                self.sends.append(remote(piece, piece, self.send_y.at[(hop - 1) * self.n_fs + step],
                                         self.recv_y.at[slot], self.me_f, self.peer(hop) * CORES + self.my_c))
                self.sends[-1].start()
            self.sends.append(remote(piece, piece, self.send_m.at[step], self.recv_m.at[slot],
                                     self.me_f, self.mate))
            self.sends[-1].start()

    def pass_dn(self):
        for hop in range(1, self.n_y):
            y = self.peer(hop)
            block = self.columns(y * CORES + self.my_c)
            copy = remote(block, block, self.dn_send_m.at[hop], self.dn_recv_m.at[y], self.me_f, self.mate)
            remote(block, block, self.dn_send_m.at[hop], self.dn_recv_y.at[y], self.me_f, self.mate).wait_recv()
            copy.start()
            self.sends.append(copy)

    def pass_second(self):
        for step in range(self.n_fs):
            f = partner(self.me_f, step, self.n_fs)
            for hop in range(1, self.n_y):
                y = self.peer(hop)
                piece = self.window(f, y, self.my_c)
                send = self.send_m.at[hop * self.n_fs + step]
                slot = y * self.n_fs + f
                remote(piece, piece, send, self.recv_y.at[slot], self.me_f, self.mate).wait_recv()
                self.sends.append(remote(piece, piece, send, self.recv_m.at[slot], self.me_f, self.mate))
                self.sends[-1].start()

    def arrive_gu(self):
        for hop in range(self.n_y):
            y = self.peer(hop)
            for step in range(self.n_fs):
                f = partner(self.me_f, step, self.n_fs)
                piece = self.window(f, y, 1 - self.my_c)
                remote(piece, piece, self.send_m.at[0], self.recv_m.at[y * self.n_fs + f],
                       self.me_f, self.mate).wait_recv()

    def arrive_dn(self):
        for hop in range(self.n_y):
            y = self.peer(hop)
            block = self.columns(y * CORES + (1 - self.my_c))
            remote(block, block, self.dn_send_m.at[0], self.dn_recv_m.at[y], self.me_f, self.mate).wait_recv()
        self.keep.wait()

    def drain(self):
        for copy in self.sends:
            copy.wait_send()
        for i in range(self.per):
            for step in range(self.n_tp):
                copy, _, _, here = self.first(i, step)
                if step == 0:
                    @pl.when(jnp.logical_not(here))
                    def _():
                        copy.wait_send()
                else:
                    copy.wait_send()


class Reduce:
    def __init__(self, ring, place, part, landing, send, recv):
        self.ring, self.part, self.landing = ring, part, landing
        self.send, self.recv = send, recv
        self.me_t = lax.axis_index("tp")
        self.goes = (ring.at(place + 1), ring.at(place - 1))
        self.share = part.shape[0] // ring.n
        self.half = part.shape[1] // 2
        self.width = self.half // CUTS
        self.sends = []

    def mine(self, way, offset, k):
        slot = self.ring.slot(offset)
        return (pl.ds(slot * self.share, self.share), pl.ds(way * self.half + k * self.width, self.width))

    def land(self, way, s, k):
        return self.landing.at[way, s, :, pl.ds(k * self.width, self.width)]

    def sem(self, way, s, k):
        return (way * (self.ring.n - 1) + s) * CUTS + k

    def arrived(self, way, s, k):
        spot, sem = self.land(way, s, k), self.sem(way, s, k)
        remote(spot, spot, self.send.at[sem], self.recv.at[sem], self.goes[way], self.me_t).wait_recv()
        return spot[...].astype(jnp.float32)

    def step(self, s):
        for k in range(CUTS):
            for way in range(2):
                rows, cols = self.mine(way, -(1 + s) if way == 0 else 1 + s, k)
                if s > 0:
                    total = self.arrived(way, s - 1, k) + self.part[rows, cols].astype(jnp.float32)
                    self.part[rows, cols] = total.astype(self.part.dtype)
                sem = self.sem(way, s, k)
                self.sends.append(remote(self.part.at[rows, cols], self.land(way, s, k), self.send.at[sem],
                                         self.recv.at[sem], self.goes[way], self.me_t))
                self.sends[-1].start()

    def last(self, store):
        for k in range(CUTS):
            for way in range(2):
                rows, cols = self.mine(way, 0, k)
                total = self.arrived(way, self.ring.n - 2, k) + self.part[rows, cols].astype(jnp.float32)
                store(cols, total)


class Gather:
    def __init__(self, ring, place, blocks, send, recv):
        self.ring, self.blocks, self.send, self.recv = ring, blocks, send, recv
        self.me_t = lax.axis_index("tp")
        self.goes = (ring.at(place + 1), ring.at(place - 1))
        self.share = blocks.shape[0] // ring.n
        self.half = blocks.shape[1] // 2
        self.far = ring.n // 2
        self.sends = []

    def spot(self, offset, k):
        slot = self.ring.slot(offset)
        return self.blocks.at[pl.ds(slot * self.share, self.share), pl.ds(k * self.half, self.half)]

    def copy(self, way, s, k):
        sign = -1 if way == 0 else 1
        sem = (way * self.far + s) * 2 + k
        return remote(self.spot(sign * s, k), self.spot(sign * (s + 1), k), self.send.at[sem],
                      self.recv.at[sem], self.goes[way], self.me_t)

    def halves(self, way, s):
        return (0, 1) if s < self.far - 1 else (way,)

    def step(self, s):
        for k in range(2):
            for way in range(2):
                if s > 0:
                    self.copy(way, s - 1, k).wait_recv()
                if k in self.halves(way, s):
                    self.sends.append(self.copy(way, s, k))
                    self.sends[-1].start()

    def last(self):
        for way in range(2):
            self.copy(way, self.far - 1, way).wait_recv()


def normalize(rows):
    return (rows * lax.rsqrt(jnp.mean(rows * rows, axis=-1, keepdims=True) + 1e-06)).astype(jnp.bfloat16)


def branch_rows(x, gu, dn, act, part, start, count):
    rows = pl.ds(start, count)
    lanes = (((1,), (1,)), ((), ()))
    for at, size in tiles(gu.shape[1], TILE):
        gate = lax.dot_general(x[rows, :], gu[0, pl.ds(at, size), :], lanes, preferred_element_type=jnp.float32)
        up = lax.dot_general(x[rows, :], gu[1, pl.ds(at, size), :], lanes, preferred_element_type=jnp.float32)
        act[:, pl.ds(at, size)] = (jax.nn.silu(gate) * up).astype(act.dtype)
    for at, size in tiles(dn.shape[1], 2 * TILE):
        part[rows, pl.ds(at, size)] = jnp.dot(
            act[...], dn[:, pl.ds(at, size)], preferred_element_type=jnp.float32
        ).astype(part.dtype)


def kernel(n_fs, n_tp, tok, gu_a, dn_a, gu_b, dn_b, gu_out_a, dn_out_a, gu_out_b, dn_out_b, done,
           x, gathered, part_a, part_b, act, mid, land_a, land_b, *sems):
    n_x = n_tp // CORES
    ring = Ring(n_fs // n_x, n_x)
    me_f, me_t = lax.axis_index("fs"), lax.axis_index("tp")
    place = ring.position(me_f // n_x, me_f % n_x)
    n, far = ring.n, ring.n // 2
    share = tok.shape[0] // n
    one = Exchange(n_fs, n_tp, gu_a, dn_a, gu_out_a, dn_out_a, sems[:11])
    two = Exchange(n_fs, n_tp, gu_b, dn_b, gu_out_b, dn_out_b, sems[11:22])
    sum_one = Reduce(ring, place, part_a, land_a, sems[22], sems[23])
    sum_two = Reduce(ring, place, part_b, land_b, sems[24], sems[25])
    spread = Gather(ring, place, gathered, sems[26], sems[27])

    barrier = pltpu.get_barrier_semaphore()

    def greet(f, t):
        pl.semaphore_signal(
            barrier, inc=1, device_id={"fs": f, "tp": t}, device_id_type=pl.DeviceIdType.MESH
        )

    holder = me_f // one.per
    is_self = holder == me_t
    for step in range(n_fs):
        f = partner(me_f, step, n_fs)
        if step == 0:
            @pl.when(jnp.logical_not(is_self))
            def _():
                greet(f, holder)
        else:
            greet(f, holder)
    for step in range(1, one.n_y):
        greet(me_f, one.peer(step) * CORES + one.my_c)
    greet(me_f, one.mate)
    greet(ring.at(place + 1), me_t)
    greet(ring.at(place - 1), me_t)
    pl.semaphore_wait(barrier, one.per * n_tp + one.n_y + 2 - jnp.where(is_self, 1, 0))

    one.start_gu()
    one.start_dn()

    @pl.loop(0, n)
    def _(j):
        sign = jnp.where(j % 2 == 0, -1, 1)
        offset = jnp.where(j < 2, j * far, sign * (j // 2))
        f = ring.at(place + offset)
        rows = tok[pl.ds(pl.multiple_of(f * share, share), share), :].astype(jnp.float32)
        x[pl.ds(pl.multiple_of(j * share, share), share), :] = normalize(rows)

    one.pass_first()
    two.start_gu()
    two.start_dn()
    one.pass_dn()
    one.pass_second()
    one.arrive_gu()
    one.arrive_dn()

    for s in range(1, far):
        branch_rows(x, gu_out_a, dn_out_a, act, part_a, 2 * s * share, 2 * share)
        sum_one.step(s - 1)
    branch_rows(x, gu_out_a, dn_out_a, act, part_a, 0, 2 * share)
    sum_one.step(far - 1)
    two.pass_first()
    for s in range(far, n - 1):
        sum_one.step(s)

    own = pl.ds(pl.multiple_of(me_f * share, share), share)

    def store_middle(cols, total):
        mid[:, cols] = (tok[own, cols].astype(jnp.float32) + 0.5 * total).astype(mid.dtype)

    sum_one.last(store_middle)
    gathered[pl.ds(0, share), :] = normalize(mid[...].astype(jnp.float32))

    spread.step(0)
    two.pass_dn()
    two.pass_second()
    two.arrive_gu()
    two.arrive_dn()
    for s in range(1, far):
        spread.step(s)
        branch_rows(gathered, gu_out_b, dn_out_b, act, part_b, 2 * s * share, 2 * share)
        sum_two.step(s - 1)
    spread.last()
    branch_rows(gathered, gu_out_b, dn_out_b, act, part_b, 0, 2 * share)
    for s in range(far - 1, n - 1):
        sum_two.step(s)

    def store_done(cols, total):
        done[:, cols] = (mid[:, cols].astype(jnp.float32) + 0.5 * total).astype(done.dtype)

    sum_two.last(store_done)

    one.drain()
    two.drain()
    for copy in sum_one.sends + spread.sends + sum_two.sends:
        copy.wait_send()


def both_half_steps(tokens, gu_a, dn_a, gu_b, dn_b):
    n_fs, n_tp = lax.axis_size("fs"), lax.axis_size("tp")
    n_y, per = n_tp // CORES, n_fs // n_tp
    count, model = tokens.shape
    share, hidden = count // n_fs, dn_a.shape[0]
    kept = tokens.dtype
    dma = pltpu.SemaphoreType.DMA
    trade = [dma((per * n_tp,)), dma((n_fs,)), dma((n_y * n_fs,)), dma((n_y * n_fs,)), dma((n_y * n_fs,)),
             dma((n_y * n_fs,)), dma, dma((n_y,)), dma((n_y,)), dma((n_y,)), dma((n_y,))]
    hops = dma((2 * (n_fs - 1) * CUTS,))
    spread = dma((2 * (n_fs // 2) * 2,))
    served = [jax.ShapeDtypeStruct((2, hidden, model), kept), jax.ShapeDtypeStruct((hidden, model), kept)]
    landing = pltpu.VMEM((2, n_fs - 1, share, model // 2), kept)
    whole = pltpu.VMEM((count, model), kept)
    return pl.pallas_call(
        functools.partial(kernel, n_fs, n_tp),
        out_shape=served + served + [jax.ShapeDtypeStruct((share, model), kept)],
        in_specs=[pl.BlockSpec(memory_space=pltpu.VMEM)] * 5,
        out_specs=[pl.BlockSpec(memory_space=pltpu.VMEM)] * 5,
        scratch_shapes=[whole, whole, whole, whole, pltpu.VMEM((2 * share, hidden), kept),
                        pltpu.VMEM((share, model), kept), landing, landing]
        + trade + trade + [hops] * 4 + [spread] * 2,
        compiler_params=pltpu.CompilerParams(
            collective_id=0, has_side_effects=True, vmem_limit_bytes=VMEM_LIMIT
        ),
        cost_estimate=pl.CostEstimate(
            flops=12 * count * model * hidden, bytes_accessed=48 * count * model, transcendentals=0
        ),
    )(tokens, gu_a, dn_a, gu_b, dn_b)


VMEM_LIMIT = 34 * 2**20


def per_device(
    prompts,
    gain_first,
    gate_first,
    up_first,
    down_first,
    gain_second,
    gate_second,
    up_second,
    down_second,
):
    def fold(gain, *matrices):
        return jnp.stack([(gain[:, None] * matrix).astype(jnp.bfloat16).T for matrix in matrices])

    tokens = prompts.reshape(-1, prompts.shape[-1])
    served_a, down_a, served_b, down_b, finished = both_half_steps(
        tokens,
        fold(gain_first, gate_first, up_first), down_first.astype(jnp.bfloat16),
        fold(gain_second, gate_second, up_second), down_second.astype(jnp.bfloat16),
    )
    return (
        served_a[0].T,
        served_a[1].T,
        down_a,
        served_b[0].T,
        served_b[1].T,
        down_b,
        finished.reshape(prompts.shape[0], -1, prompts.shape[-1]),
    )


def solution(mesh):
    in_specs = (
        P("tp", None, None),
        P("fs"),
        P("fs", "tp"),
        P("fs", "tp"),
        P("fs", "tp"),
        P("fs"),
        P("fs", "tp"),
        P("fs", "tp"),
        P("fs", "tp"),
    )
    out_specs = (
        P(None, "fs"),
        P(None, "fs"),
        P("fs", None),
        P(None, "fs"),
        P(None, "fs"),
        P("fs", None),
        P("tp", "fs", None),
    )
    return jax.shard_map(
        per_device, mesh=mesh, in_specs=in_specs, out_specs=out_specs, check_vma=False
    )
```

profile of v0, /device:TPU:0, one launch (start us, length us, event | category | flops | bytes accessed | tf_op | source)
XLA Modules:
  0.0 301.3 jit_solution(6237145618808541879)
XLA Ops:
  0.6 0.0 copy-start.1
  0.6 1.6 convert_element_type.20.dn_a
  2.2 0.2 copy-done.1
  2.4 0.1 convert_element_type.23.dn_b
  2.5 1.8 copy.16
  4.3 0.0 copy-start.2
  4.3 2.9 copy.17
  7.2 0.0 copy-done.2
  7.2 1.6 fusion
  8.8 0.1 pad_maximum_fusion.gu_a
  9.0 2.9 copy.18
  11.9 0.0 copy-start.3
  11.9 2.9 copy.19
  14.8 0.0 copy-done.3
  14.8 0.0 copy-start
  14.8 2.2 fusion.2
  17.0 0.1 pad_maximum_fusion.1.gu_b
  17.1 0.7 copy-done
  17.9 273.1 %shard_map.144 = (bf16[2,704,2048]{2,1,0:T(8,128)(2,1)S(1)}, bf16[704,2048]{1,0:T(8,128)(2,1)S(1)}, bf16[2,704,2048]{2,1,0:T(8,128)(2,1)}, bf16[704,2048]{1,0:T(8,128)(2,1)S(1)}, bf16[128,2048]{1,0:T(8,128)(2,1)S(1)}) custom-call(bf16[1024,2048]{1,0:T(8,128)(2,1)S(1)} %bitcast.35, bf16[2,1408,256]{2,1,0:T(8,128)(2,1)S(1)} %pad_maximum_fusion.gu_a, ...), custom_call_target="tpu_custom_call" | custom-call | flops 17716740096 | bytes 100663296 | tf_op jit(solution)/shard_map/pallas_call | solution.py:406
  291.0 6.3 %slice_bitcast_fusion = (bf16[2048,704]{0,1:T(8,128)(2,1)}, bf16[2048,704]{0,1:T(8,128)(2,1)}, bf16[2048,704]{0,1:T(8,128)(2,1)}, bf16[2048,704]{0,1:T(8,128)(2,1)}) fusion(bf16[2,704,2048]{2,1,0:T(8,128)(2,1)} %get-tuple-element.14, bf16[2,704,2048]{2,1,0:T(8,128)(2,1)S(1)} %get-tuple-element.12), kind=kLoop, calls=%fused_computation | loop fusion | bytes 23068672 | tf_op jit(solution)/shard_map/transpose | solution.py:451
  297.3 1.6 copy.23
  298.9 1.6 copy.24
  300.5 0.8 copy.25
Async XLA Ops:
  0.6 1.8 copy-start.1
  4.3 2.9 copy-start.2
  11.9 2.9 copy-start.3
  14.8 3.1 %copy-start = (bf16[1,1024,2048]{2,1,0:T(8,128)(2,1)S(1)}, bf16[1,1024,2048]{2,1,0:T(8,128)(2,1)}, u32[]{:S(2)}) copy-start(bf16[1,1024,2048]{2,1,0:T(8,128)(2,1)} %param.9) | copy-start | bytes 12582916
where the time goes:
time: 302 us; the launch traced here: 301 us
  Pallas kernels  273 us (90%)
  local copies, waits for them, and re-layouts  21.7 us (7%)
  other arithmetic  5.7 us (2%)
    pallas_call x1, Pallas kernels, both_half_steps(): pl.pallas_call(functools.partial(kernel, n_fs, n_tp), out_shape=served +...  273 us
    unnamed x15, local copies, waits for them, and re-layouts  15.4 us
    transpose x1, local copies, waits for them, and re-layouts, per_device(): served_b[1]  6.3 us

commit v1 on v0

--- a/solution.py
+++ b/solution.py
@@ -65,100 +65,134 @@
 
 
 class Exchange:
-    def __init__(self, n_fs, n_tp, gu, dn, gu_out, dn_out, sems):
-        (self.send_a, self.recv_a, self.send_y, self.recv_y, self.send_m, self.recv_m,
-         self.dn_local, self.dn_send_y, self.dn_recv_y, self.dn_send_m, self.dn_recv_m) = sems
+    def __init__(self, n_fs, n_tp, gu, dn, gu_out, dn_out, bounce, sems):
+        (self.send_c, self.recv_c, self.send_n, self.send_f, self.recv_a, self.send_y, self.recv_y,
+         self.send_m, self.recv_m, self.dn_local, self.dn_send_y, self.dn_recv_y, self.dn_send_m,
+         self.dn_recv_m) = sems
         self.n_fs, self.n_tp, self.n_y = n_fs, n_tp, n_tp // CORES
         self.per = n_fs // n_tp
-        self.gu, self.dn, self.gu_out, self.dn_out = gu, dn, gu_out, dn_out
+        self.gu, self.dn, self.gu_out, self.dn_out, self.bounce = gu, dn, gu_out, dn_out, bounce
         self.hidden, self.rows = gu.shape[1] // self.per, gu.shape[2]
         self.part = self.hidden // self.n_y
         self.me_f, self.me_t = lax.axis_index("fs"), lax.axis_index("tp")
         self.my_y, self.my_c = self.me_t // CORES, self.me_t % CORES
         self.mate = self.my_y * CORES + (1 - self.my_c)
-        self.sends = []
+        self.at_home = self.me_f // self.per // CORES == self.my_y
 
     def peer(self, step):
         return (self.my_y + step) % self.n_y
+
+    def beside(self, step):
+        return self.peer(step) * CORES + self.my_c
 
     def window(self, f, y, c):
         return self.gu_out.at[c, pl.ds(pl.multiple_of(y * self.part, 8), self.part),
                               pl.ds(pl.multiple_of(f * self.rows, 128), self.rows)]
 
-    def first(self, i, step):
-        q = (self.me_t + step) % self.n_tp
-        y, c = q // CORES, q % CORES
-        f = self.me_t * self.per + i
-        src = self.gu.at[c, pl.ds(pl.multiple_of(i * self.hidden + y * self.part, 8), self.part), :]
-        dst = self.window(self.me_f, y, c)
-        copy = remote(src, dst, self.send_a.at[i * self.n_tp + step], self.recv_a.at[self.me_f], f, q)
-        return copy, src, dst, f == self.me_f
-
-    def start_gu(self):
-        for step in range(self.n_tp - 1, -1, -1):
+    def own(self, kind, i, y):
+        return self.gu.at[kind, pl.ds(pl.multiple_of(i * self.hidden + y * self.part, 8), self.part), :]
+
+    def cross(self, hop, kind, i):
+        sem = ((hop - 1) * 2 + kind) * self.per + i
+        return remote(self.own(kind, i, self.peer(hop)), self.bounce.at[hop - 1, kind, i],
+                      self.send_c.at[sem], self.recv_c.at[sem], self.me_f, self.beside(hop))
+
+    def start_cross(self, kind):
+        for hop in range(1, self.n_y):
             for i in range(self.per):
-                copy, src, dst, here = self.first(i, step)
-                if step == 0:
-                    @pl.when(here)
-                    def _():
-                        pltpu.make_async_copy(src, dst, self.recv_a.at[self.me_f]).start()
-
-                    @pl.when(jnp.logical_not(here))
-                    def _():
-                        copy.start()
-                else:
-                    copy.start()
+                self.cross(hop, kind, i).start()
+
+    def deliver(self, src, send, t, kind, i, act):
+        f = t * self.per + i
+        dst = self.window(self.me_f, self.my_y, kind)
+        recv = self.recv_a.at[self.me_f]
+        here = jnp.logical_and(f == self.me_f, kind == self.my_c)
+
+        @pl.when(jnp.logical_not(here))
+        def _():
+            copy = remote(src, dst, send, recv, f, self.my_y * CORES + kind)
+            copy.start() if act else copy.wait_send()
+
+        if act:
+            @pl.when(here)
+            def _():
+                pltpu.make_async_copy(src, dst, recv).start()
+
+    def near(self, kind, act=True):
+        for i in range(self.per):
+            self.deliver(self.own(kind, i, self.my_y), self.send_n.at[kind * self.per + i], self.me_t,
+                         kind, i, act)
+
+    def pass_cross(self, act=True):
+        for kind in range(2):
+            for hop in range(1, self.n_y):
+                for i in range(self.per):
+                    sem = ((hop - 1) * 2 + kind) * self.per + i
+                    held = self.bounce.at[self.n_y - hop - 1, kind, i]
+                    came = ((self.n_y - hop - 1) * 2 + kind) * self.per + i
+                    if act:
+                        remote(held, held, self.send_c.at[came], self.recv_c.at[came], self.me_f,
+                               self.mate).wait_recv()
+                    self.deliver(held, self.send_f.at[sem], self.beside(hop), kind, i, act)
 
     def columns(self, t):
         width = self.dn.shape[1]
         return self.dn_out.at[:, pl.ds(pl.multiple_of(t * width, 128), width)]
 
+    def dn_first(self):
+        mine = self.columns(self.me_t)
+        copies = [remote(self.dn, mine, self.dn_send_y.at[step], self.dn_recv_y.at[self.my_y],
+                         self.me_f, self.beside(step)) for step in range(1, self.n_y)]
+        copies.append(remote(self.dn, mine, self.dn_send_m.at[0], self.dn_recv_m.at[self.my_y],
+                             self.me_f, self.mate))
+        return copies
+
     def start_dn(self):
-        mine = self.columns(self.me_t)
-        self.keep = pltpu.make_async_copy(self.dn, mine, self.dn_local)
+        self.keep = pltpu.make_async_copy(self.dn, self.columns(self.me_t), self.dn_local)
         self.keep.start()
-        for step in range(1, self.n_y):
-            self.sends.append(remote(self.dn, mine, self.dn_send_y.at[step], self.dn_recv_y.at[self.my_y],
-                                     self.me_f, self.peer(step) * CORES + self.my_c))
-            self.sends[-1].start()
-        self.sends.append(remote(self.dn, mine, self.dn_send_m.at[0], self.dn_recv_m.at[self.my_y],
-                                 self.me_f, self.mate))
-        self.sends[-1].start()
+        for copy in self.dn_first():
+            copy.start()
+
+    def on_first(self, step):
+        f = partner(self.me_f, step, self.n_fs)
+        piece = self.window(f, self.my_y, self.my_c)
+        slot = self.my_y * self.n_fs + f
+        copies = [remote(piece, piece, self.send_y.at[(hop - 1) * self.n_fs + step], self.recv_y.at[slot],
+                         self.me_f, self.beside(hop)) for hop in range(1, self.n_y)]
+        copies.append(remote(piece, piece, self.send_m.at[step], self.recv_m.at[slot], self.me_f, self.mate))
+        return f, piece, copies
 
     def pass_first(self):
         for step in range(self.n_fs):
-            f = partner(self.me_f, step, self.n_fs)
-            piece = self.window(f, self.my_y, self.my_c)
-            slot = self.my_y * self.n_fs + f
+            f, piece, copies = self.on_first(step)
             remote(piece, piece, self.send_m.at[0], self.recv_a.at[f], self.me_f, self.mate).wait_recv()
-            for hop in range(1, self.n_y):
-                self.sends.append(remote(piece, piece, self.send_y.at[(hop - 1) * self.n_fs + step],
-                                         self.recv_y.at[slot], self.me_f, self.peer(hop) * CORES + self.my_c))
-                self.sends[-1].start()
-            self.sends.append(remote(piece, piece, self.send_m.at[step], self.recv_m.at[slot],
-                                     self.me_f, self.mate))
-            self.sends[-1].start()
+            for copy in copies:
+                copy.start()
+
+    def on_dn(self, hop):
+        y = self.peer(hop)
+        block = self.columns(y * CORES + self.my_c)
+        return y, block, remote(block, block, self.dn_send_m.at[hop], self.dn_recv_m.at[y], self.me_f, self.mate)
 
     def pass_dn(self):
         for hop in range(1, self.n_y):
-            y = self.peer(hop)
-            block = self.columns(y * CORES + self.my_c)
-            copy = remote(block, block, self.dn_send_m.at[hop], self.dn_recv_m.at[y], self.me_f, self.mate)
+            y, block, copy = self.on_dn(hop)
             remote(block, block, self.dn_send_m.at[hop], self.dn_recv_y.at[y], self.me_f, self.mate).wait_recv()
             copy.start()
-            self.sends.append(copy)
+
+    def on_second(self, step, hop):
+        f, y = partner(self.me_f, step, self.n_fs), self.peer(hop)
+        piece = self.window(f, y, self.my_c)
+        slot = y * self.n_fs + f
+        send = self.send_m.at[hop * self.n_fs + step]
+        return slot, piece, send, remote(piece, piece, send, self.recv_m.at[slot], self.me_f, self.mate)
 
     def pass_second(self):
         for step in range(self.n_fs):
-            f = partner(self.me_f, step, self.n_fs)
             for hop in range(1, self.n_y):
-                y = self.peer(hop)
-                piece = self.window(f, y, self.my_c)
-                send = self.send_m.at[hop * self.n_fs + step]
-                slot = y * self.n_fs + f
+                slot, piece, send, copy = self.on_second(step, hop)
                 remote(piece, piece, send, self.recv_y.at[slot], self.me_f, self.mate).wait_recv()
-                self.sends.append(remote(piece, piece, send, self.recv_m.at[slot], self.me_f, self.mate))
-                self.sends[-1].start()
+                copy.start()
 
     def arrive_gu(self):
         for hop in range(self.n_y):
@@ -177,17 +211,17 @@
         self.keep.wait()
 
     def drain(self):
-        for copy in self.sends:
+        for kind in range(2):
+            for hop in range(1, self.n_y):
+                for i in range(self.per):
+                    self.cross(hop, kind, i).wait_send()
+            self.near(kind, False)
+        self.pass_cross(False)
+        copies = self.dn_first() + [self.on_dn(hop)[2] for hop in range(1, self.n_y)]
+        for step in range(self.n_fs):
+            copies += self.on_first(step)[2] + [self.on_second(step, hop)[3] for hop in range(1, self.n_y)]
+        for copy in copies:
             copy.wait_send()
-        for i in range(self.per):
-            for step in range(self.n_tp):
-                copy, _, _, here = self.first(i, step)
-                if step == 0:
-                    @pl.when(jnp.logical_not(here))
-                    def _():
-                        copy.wait_send()
-                else:
-                    copy.wait_send()
 
 
 class Reduce:
@@ -290,19 +324,45 @@
         ).astype(part.dtype)
 
 
-def kernel(n_fs, n_tp, tok, gu_a, dn_a, gu_b, dn_b, gu_out_a, dn_out_a, gu_out_b, dn_out_b, done,
-           x, gathered, part_a, part_b, act, mid, land_a, land_b, *sems):
+def fold(staged, gain, kind, gu):
+    count = staged.shape[2]
+
+    def turn(cols, size):
+        gu[kind, pl.ds(cols, size), :] = (staged[kind, :, pl.ds(cols, size)].T * gain[...]).astype(gu.dtype)
+
+    @pl.loop(0, count // LANES)
+    def _(j):
+        turn(pl.multiple_of(j * LANES, LANES), LANES)
+
+    if count % LANES:
+        turn(count - count % LANES, count % LANES)
+
+
+def kernel(n_fs, n_tp, tok, gain_a, gain_b, gate_a, up_a, down_a, gate_b, up_b, down_b,
+           gu_out_a, dn_out_a, gu_out_b, dn_out_b, done,
+           staged, staged_dn, gu_a, gu_b, dn_a, dn_b, bounce_a, bounce_b,
+           x, part, act, mid, landing, load_sems, *sems):
     n_x = n_tp // CORES
     ring = Ring(n_fs // n_x, n_x)
     me_f, me_t = lax.axis_index("fs"), lax.axis_index("tp")
     place = ring.position(me_f // n_x, me_f % n_x)
     n, far = ring.n, ring.n // 2
     share = tok.shape[0] // n
-    one = Exchange(n_fs, n_tp, gu_a, dn_a, gu_out_a, dn_out_a, sems[:11])
-    two = Exchange(n_fs, n_tp, gu_b, dn_b, gu_out_b, dn_out_b, sems[11:22])
-    sum_one = Reduce(ring, place, part_a, land_a, sems[22], sems[23])
-    sum_two = Reduce(ring, place, part_b, land_b, sems[24], sems[25])
-    spread = Gather(ring, place, gathered, sems[26], sems[27])
+    each = TRADE_SEMS
+    one = Exchange(n_fs, n_tp, gu_a, dn_a, gu_out_a, dn_out_a, bounce_a, sems[:each])
+    two = Exchange(n_fs, n_tp, gu_b, dn_b, gu_out_b, dn_out_b, bounce_b, sems[each:2 * each])
+    rest = sems[2 * each:]
+    sum_one = Reduce(ring, place, part, landing, rest[0], rest[1])
+    sum_two = Reduce(ring, place, part, landing, rest[2], rest[3])
+    spread = Gather(ring, place, x, rest[4], rest[5])
+
+    def load(step, gate, up, down):
+        return [pltpu.make_async_copy(src, dst, load_sems.at[3 * step + i])
+                for i, (src, dst) in enumerate(((gate, staged.at[0]), (up, staged.at[1]), (down, staged_dn)))]
+
+    loads = load(0, gate_a, up_a, down_a)
+    for copy in loads:
+        copy.start()
 
     barrier = pltpu.get_barrier_semaphore()
 
@@ -311,25 +371,34 @@
             barrier, inc=1, device_id={"fs": f, "tp": t}, device_id_type=pl.DeviceIdType.MESH
         )
 
-    holder = me_f // one.per
-    is_self = holder == me_t
+    core = me_f // one.per % CORES
+    is_self = core == one.my_c
     for step in range(n_fs):
         f = partner(me_f, step, n_fs)
         if step == 0:
             @pl.when(jnp.logical_not(is_self))
             def _():
-                greet(f, holder)
+                greet(f, one.my_y * CORES + core)
         else:
-            greet(f, holder)
+            greet(f, one.my_y * CORES + core)
     for step in range(1, one.n_y):
-        greet(me_f, one.peer(step) * CORES + one.my_c)
+        greet(me_f, one.beside(step))
     greet(me_f, one.mate)
     greet(ring.at(place + 1), me_t)
     greet(ring.at(place - 1), me_t)
-    pl.semaphore_wait(barrier, one.per * n_tp + one.n_y + 2 - jnp.where(is_self, 1, 0))
-
-    one.start_gu()
+    pl.semaphore_wait(barrier, n_fs + one.n_y + 2 - jnp.where(is_self, 1, 0))
+
+    for kind in range(2):
+        loads[kind].wait()
+        fold(staged, gain_a, kind, gu_a)
+        one.start_cross(kind)
+        one.near(kind)
+    loads[2].wait()
+    dn_a[...] = staged_dn[...].astype(dn_a.dtype)
     one.start_dn()
+    loads = load(1, gate_b, up_b, down_b)
+    for copy in loads:
+        copy.start()
 
     @pl.loop(0, n)
     def _(j):
@@ -339,20 +408,40 @@
         rows = tok[pl.ds(pl.multiple_of(f * share, share), share), :].astype(jnp.float32)
         x[pl.ds(pl.multiple_of(j * share, share), share), :] = normalize(rows)
 
+    one.pass_cross()
+    for kind in range(2):
+        loads[kind].wait()
+        fold(staged, gain_b, kind, gu_b)
+        two.near(kind)
+    loads[2].wait()
+    dn_b[...] = staged_dn[...].astype(dn_b.dtype)
+
     one.pass_first()
-    two.start_gu()
-    two.start_dn()
+    two.start_cross(0)
+    two.start_cross(1)
     one.pass_dn()
     one.pass_second()
     one.arrive_gu()
     one.arrive_dn()
 
+    @pl.when(two.at_home)
+    def _():
+        two.pass_first()
+
+    two.start_dn()
+
     for s in range(1, far):
-        branch_rows(x, gu_out_a, dn_out_a, act, part_a, 2 * s * share, 2 * share)
+        branch_rows(x, gu_out_a, dn_out_a, act, part, 2 * s * share, 2 * share)
         sum_one.step(s - 1)
-    branch_rows(x, gu_out_a, dn_out_a, act, part_a, 0, 2 * share)
+        if s == 1:
+            two.pass_cross()
+    branch_rows(x, gu_out_a, dn_out_a, act, part, 0, 2 * share)
     sum_one.step(far - 1)
-    two.pass_first()
+
+    @pl.when(jnp.logical_not(two.at_home))
+    def _():
+        two.pass_first()
+
     for s in range(far, n - 1):
         sum_one.step(s)
 
@@ -362,19 +451,23 @@
         mid[:, cols] = (tok[own, cols].astype(jnp.float32) + 0.5 * total).astype(mid.dtype)
 
     sum_one.last(store_middle)
-    gathered[pl.ds(0, share), :] = normalize(mid[...].astype(jnp.float32))
+    x[pl.ds(0, share), :] = normalize(mid[...].astype(jnp.float32))
 
     spread.step(0)
     two.pass_dn()
+    for copy in sum_one.sends:
+        copy.wait_send()
+    spread.step(1)
     two.pass_second()
     two.arrive_gu()
     two.arrive_dn()
     for s in range(1, far):
-        spread.step(s)
-        branch_rows(gathered, gu_out_b, dn_out_b, act, part_b, 2 * s * share, 2 * share)
+        if s > 1:
+            spread.step(s)
+        branch_rows(x, gu_out_b, dn_out_b, act, part, 2 * s * share, 2 * share)
         sum_two.step(s - 1)
     spread.last()
-    branch_rows(gathered, gu_out_b, dn_out_b, act, part_b, 0, 2 * share)
+    branch_rows(x, gu_out_b, dn_out_b, act, part, 0, 2 * share)
     for s in range(far - 1, n - 1):
         sum_two.step(s)
 
@@ -385,42 +478,77 @@
 
     one.drain()
     two.drain()
-    for copy in sum_one.sends + spread.sends + sum_two.sends:
+    for copy in spread.sends + sum_two.sends:
         copy.wait_send()
 
 
-def both_half_steps(tokens, gu_a, dn_a, gu_b, dn_b):
+TRADE_SEMS = 14
+LANES = 128
+VMEM_LIMIT = 32 * 2**20
+
+
+def stay(array):
+    return pltpu.with_memory_space_constraint(array, pltpu.HBM)
+
+
+def both_half_steps(tokens, gains, first, second):
     n_fs, n_tp = lax.axis_size("fs"), lax.axis_size("tp")
     n_y, per = n_tp // CORES, n_fs // n_tp
     count, model = tokens.shape
-    share, hidden = count // n_fs, dn_a.shape[0]
+    rows, wide = first[0].shape
+    share, hidden = count // n_fs, wide // per
     kept = tokens.dtype
     dma = pltpu.SemaphoreType.DMA
-    trade = [dma((per * n_tp,)), dma((n_fs,)), dma((n_y * n_fs,)), dma((n_y * n_fs,)), dma((n_y * n_fs,)),
-             dma((n_y * n_fs,)), dma, dma((n_y,)), dma((n_y,)), dma((n_y,)), dma((n_y,))]
+    hop, every = dma(((n_y - 1) * 2 * per,)), dma((n_y * n_fs,))
+    trade = [hop, hop, dma((2 * per,)), hop, dma((n_fs,)), every, every, every, every, dma, dma((n_y,)),
+             dma((n_y,)), dma((n_y,)), dma((n_y,))]
     hops = dma((2 * (n_fs - 1) * CUTS,))
     spread = dma((2 * (n_fs // 2) * 2,))
     served = [jax.ShapeDtypeStruct((2, hidden, model), kept), jax.ShapeDtypeStruct((hidden, model), kept)]
-    landing = pltpu.VMEM((2, n_fs - 1, share, model // 2), kept)
-    whole = pltpu.VMEM((count, model), kept)
+    vmem = pltpu.VMEM
+    folded, down = vmem((2, wide, rows), kept), vmem(first[2].shape, kept)
+    bounce = vmem((n_y - 1, 2, per, hidden // n_y, rows), kept)
     return pl.pallas_call(
         functools.partial(kernel, n_fs, n_tp),
         out_shape=served + served + [jax.ShapeDtypeStruct((share, model), kept)],
-        in_specs=[pl.BlockSpec(memory_space=pltpu.VMEM)] * 5,
-        out_specs=[pl.BlockSpec(memory_space=pltpu.VMEM)] * 5,
-        scratch_shapes=[whole, whole, whole, whole, pltpu.VMEM((2 * share, hidden), kept),
-                        pltpu.VMEM((share, model), kept), landing, landing]
-        + trade + trade + [hops] * 4 + [spread] * 2,
+        in_specs=[pl.BlockSpec(memory_space=vmem)] * 3 + [pl.BlockSpec(memory_space=pltpu.HBM)] * 6,
+        out_specs=[pl.BlockSpec(memory_space=vmem)] * 5,
+        scratch_shapes=[
+            vmem((2, rows, wide), first[0].dtype), vmem(first[2].shape, first[2].dtype),
+            folded, folded, down, down, bounce, bounce,
+            vmem((count, model), kept), vmem((count, model), kept), vmem((2 * share, hidden), kept),
+            vmem((share, model), kept), vmem((2, n_fs - 1, share, model // 2), kept), dma((6,)),
+        ] + trade + trade + [hops] * 4 + [spread] * 2,
         compiler_params=pltpu.CompilerParams(
             collective_id=0, has_side_effects=True, vmem_limit_bytes=VMEM_LIMIT
         ),
         cost_estimate=pl.CostEstimate(
             flops=12 * count * model * hidden, bytes_accessed=48 * count * model, transcendentals=0
         ),
-    )(tokens, gu_a, dn_a, gu_b, dn_b)
-
-
-VMEM_LIMIT = 34 * 2**20
+    )(tokens, *gains, *map(stay, first + second))
+
+
+def place_kernel(gu_a, dn_a, gu_b, dn_b, done, *refs):
+    outs, sems = refs[:-1], refs[-1]
+    sources = (gu_a.at[0], gu_a.at[1], dn_a, gu_b.at[0], gu_b.at[1], dn_b, done)
+    copies = [pltpu.make_async_copy(src, dst, sems.at[i]) for i, (src, dst) in enumerate(zip(sources, outs))]
+    for copy in copies:
+        copy.start()
+    for copy in copies:
+        copy.wait()
+
+
+def place_results(gu_a, dn_a, gu_b, dn_b, done):
+    block = jax.ShapeDtypeStruct(dn_a.shape, dn_a.dtype)
+    outs = [block] * 6 + [jax.ShapeDtypeStruct(done.shape, done.dtype)]
+    return pl.pallas_call(
+        place_kernel,
+        out_shape=outs,
+        in_specs=[pl.BlockSpec(memory_space=pltpu.VMEM)] * 5,
+        out_specs=[pl.BlockSpec(memory_space=pltpu.HBM)] * 7,
+        scratch_shapes=[pltpu.SemaphoreType.DMA((7,))],
+        compiler_params=pltpu.CompilerParams(vmem_limit_bytes=2**20),
+    )(gu_a, dn_a, gu_b, dn_b, done)
 
 
 def per_device(
@@ -434,21 +562,17 @@
     up_second,
     down_second,
 ):
-    def fold(gain, *matrices):
-        return jnp.stack([(gain[:, None] * matrix).astype(jnp.bfloat16).T for matrix in matrices])
-
     tokens = prompts.reshape(-1, prompts.shape[-1])
-    served_a, down_a, served_b, down_b, finished = both_half_steps(
-        tokens,
-        fold(gain_first, gate_first, up_first), down_first.astype(jnp.bfloat16),
-        fold(gain_second, gate_second, up_second), down_second.astype(jnp.bfloat16),
-    )
+    gate_a, up_a, down_a, gate_b, up_b, down_b, finished = place_results(*both_half_steps(
+        tokens, (gain_first[None], gain_second[None]),
+        (gate_first, up_first, down_first), (gate_second, up_second, down_second),
+    ))
     return (
-        served_a[0].T,
-        served_a[1].T,
+        gate_a.T,
+        up_a.T,
         down_a,
-        served_b[0].T,
-        served_b[1].T,
+        gate_b.T,
+        up_b.T,
         down_b,
         finished.reshape(prompts.shape[0], -1, prompts.shape[-1]),
     )

time: 302 us -> 240 us (0.79)
  Pallas kernels: 273 us -> 236 us
  local copies, waits for them, and re-layouts: 21.7 us -> 3.54 us
  other arithmetic: 5.7 us -> 0 us
    pallas_call x1, Pallas kernels: 273 us -> 230 us  [both_half_steps(): pl.pallas_call(functools.partial(kernel, n_fs, n_tp), out_shape=served +...]
    unnamed x15 -> x6, local copies, waits for them, and re-layouts: 15.4 us -> 3.54 us
    transpose x1 -> x0, local copies, waits for them, and re-layouts: 6.3 us -> none  [per_device(): served_b[1]]
    pallas_call x0 -> x1, Pallas kernels: none -> 6.22 us  [place_results(): pl.pallas_call(place_kernel, out_shape=outs, in_specs=[pl.BlockSpec(memor...]
    another operation x4 -> x0, other arithmetic: 4.05 us -> none  [fold(): jnp.stack([(gain[:, None] * matrix).astype(jnp.bfloat16).T for matrix in...]
where the time goes in v1:
time: 240 us
  Pallas kernels  236 us (98%)
  local copies, waits for them, and re-layouts  3.54 us (1%)
    pallas_call x1, Pallas kernels, both_half_steps(): pl.pallas_call(functools.partial(kernel, n_fs, n_tp), out_shape=served +...  230 us
    pallas_call x1, Pallas kernels, place_results(): pl.pallas_call(place_kernel, out_shape=outs, in_specs=[pl.BlockSpec(memor...  6.22 us

profile of v1, /device:TPU:0, one launch (start us, length us, event | category | flops | bytes accessed | tf_op | source)
XLA Modules:
  0.0 240.3 jit_solution(13095963342024541282)
XLA Ops:
  0.6 0.0 copy-start
  0.6 2.2 copy-done
  2.8 0.0 copy-start.1
  2.8 0.7 copy-done.1
  3.5 0.0 copy-start.2
  3.5 0.7 copy-done.2
  4.2 229.7 %shard_map.144 = (bf16[2,704,2048]{2,1,0:T(8,128)(2,1)S(1)}, bf16[704,2048]{1,0:T(8,128)(2,1)S(1)}, bf16[2,704,2048]{2,1,0:T(8,128)(2,1)S(1)}, bf16[704,2048]{1,0:T(8,128)(2,1)S(1)}, bf16[128,2048]{1,0:T(8,128)(2,1)S(1)}) custom-call(bf16[1024,2048]{1,0:T(8,128)(2,1)S(1)} %bitcast.8, f32[1,256]{1,0:T(1,128)S(1)} %bitcast.9, f32[1,256]{1,0:T(1,128)S(1)} %bitcast.10, ...), custom_call_target="tpu_custom_call" | custom-call | flops 17716740096 | bytes 100663296 | tf_op jit(solution)/shard_map/pallas_call | solution.py:511
  233.9 6.2 %shard_map.145 = (bf16[704,2048]{1,0:T(8,128)(2,1)}, bf16[704,2048]{1,0:T(8,128)(2,1)}, bf16[704,2048]{1,0:T(8,128)(2,1)}, bf16[704,2048]{1,0:T(8,128)(2,1)}, bf...) custom-call(bf16[2,704,2048]{2,1,0:T(8,128)(2,1)S(1)} %get-tuple-element.19.gu_a, ...), custom_call_target="tpu_custom_call" | custom-call | tf_op jit(solution)/shard_map/pallas_call | solution.py:544
Async XLA Ops:
  0.6 2.2 copy-start
  2.8 0.7 copy-start.1
  3.5 0.7 copy-start.2

commit v2 on v1

--- a/solution.py
+++ b/solution.py
@@ -162,8 +162,8 @@
         copies.append(remote(piece, piece, self.send_m.at[step], self.recv_m.at[slot], self.me_f, self.mate))
         return f, piece, copies
 
-    def pass_first(self):
-        for step in range(self.n_fs):
+    def pass_first(self, steps):
+        for step in steps:
             f, piece, copies = self.on_first(step)
             remote(piece, piece, self.send_m.at[0], self.recv_a.at[f], self.me_f, self.mate).wait_recv()
             for copy in copies:
@@ -311,16 +311,20 @@
     return (rows * lax.rsqrt(jnp.mean(rows * rows, axis=-1, keepdims=True) + 1e-06)).astype(jnp.bfloat16)
 
 
-def branch_rows(x, gu, dn, act, part, start, count):
+def active_rows(x, gu, act, start, count):
     rows = pl.ds(start, count)
     lanes = (((1,), (1,)), ((), ()))
     for at, size in tiles(gu.shape[1], TILE):
         gate = lax.dot_general(x[rows, :], gu[0, pl.ds(at, size), :], lanes, preferred_element_type=jnp.float32)
         up = lax.dot_general(x[rows, :], gu[1, pl.ds(at, size), :], lanes, preferred_element_type=jnp.float32)
-        act[:, pl.ds(at, size)] = (jax.nn.silu(gate) * up).astype(act.dtype)
+        act[rows, pl.ds(at, size)] = (jax.nn.silu(gate) * up).astype(act.dtype)
+
+
+def down_rows(act, dn, part, start, count):
+    rows = pl.ds(start, count)
     for at, size in tiles(dn.shape[1], 2 * TILE):
         part[rows, pl.ds(at, size)] = jnp.dot(
-            act[...], dn[:, pl.ds(at, size)], preferred_element_type=jnp.float32
+            act[rows, :], dn[:, pl.ds(at, size)], preferred_element_type=jnp.float32
         ).astype(part.dtype)
 
 
@@ -395,7 +399,6 @@
         one.near(kind)
     loads[2].wait()
     dn_a[...] = staged_dn[...].astype(dn_a.dtype)
-    one.start_dn()
     loads = load(1, gate_b, up_b, down_b)
     for copy in loads:
         copy.start()
@@ -408,41 +411,35 @@
         rows = tok[pl.ds(pl.multiple_of(f * share, share), share), :].astype(jnp.float32)
         x[pl.ds(pl.multiple_of(j * share, share), share), :] = normalize(rows)
 
-    one.pass_cross()
     for kind in range(2):
         loads[kind].wait()
         fold(staged, gain_b, kind, gu_b)
+        two.start_cross(kind)
         two.near(kind)
     loads[2].wait()
     dn_b[...] = staged_dn[...].astype(dn_b.dtype)
 
-    one.pass_first()
-    two.start_cross(0)
-    two.start_cross(1)
-    one.pass_dn()
+    one.pass_cross()
+    one.pass_first(range(n_fs // 2))
+    two.pass_cross()
+    one.pass_first(range(n_fs // 2, n_fs))
+    one.start_dn()
     one.pass_second()
     one.arrive_gu()
+
+    @pl.loop(0, far)
+    def _(j):
+        active_rows(x, gu_out_a, act, pl.multiple_of(j * 2 * share, 2 * share), 2 * share)
+
+    two.pass_first(range(n_fs))
+    two.start_dn()
+    one.pass_dn()
     one.arrive_dn()
-
-    @pl.when(two.at_home)
-    def _():
-        two.pass_first()
-
-    two.start_dn()
-
     for s in range(1, far):
-        branch_rows(x, gu_out_a, dn_out_a, act, part, 2 * s * share, 2 * share)
+        down_rows(act, dn_out_a, part, 2 * s * share, 2 * share)
         sum_one.step(s - 1)
-        if s == 1:
-            two.pass_cross()
-    branch_rows(x, gu_out_a, dn_out_a, act, part, 0, 2 * share)
-    sum_one.step(far - 1)
-
-    @pl.when(jnp.logical_not(two.at_home))
-    def _():
-        two.pass_first()
-
-    for s in range(far, n - 1):
+    down_rows(act, dn_out_a, part, 0, 2 * share)
+    for s in range(far - 1, n - 1):
         sum_one.step(s)
 
     own = pl.ds(pl.multiple_of(me_f * share, share), share)
@@ -464,10 +461,12 @@
     for s in range(1, far):
         if s > 1:
             spread.step(s)
-        branch_rows(x, gu_out_b, dn_out_b, act, part, 2 * s * share, 2 * share)
+        active_rows(x, gu_out_b, act, 2 * s * share, 2 * share)
+        down_rows(act, dn_out_b, part, 2 * s * share, 2 * share)
         sum_two.step(s - 1)
     spread.last()
-    branch_rows(x, gu_out_b, dn_out_b, act, part, 0, 2 * share)
+    active_rows(x, gu_out_b, act, 0, 2 * share)
+    down_rows(act, dn_out_b, part, 0, 2 * share)
     for s in range(far - 1, n - 1):
         sum_two.step(s)
 
@@ -516,7 +515,7 @@
         scratch_shapes=[
             vmem((2, rows, wide), first[0].dtype), vmem(first[2].shape, first[2].dtype),
             folded, folded, down, down, bounce, bounce,
-            vmem((count, model), kept), vmem((count, model), kept), vmem((2 * share, hidden), kept),
+            vmem((count, model), kept), vmem((count, model), kept), vmem((count, hidden), kept),
             vmem((share, model), kept), vmem((2, n_fs - 1, share, model // 2), kept), dma((6,)),
         ] + trade + trade + [hops] * 4 + [spread] * 2,
         compiler_params=pltpu.CompilerParams(

time: 240 us -> 228 us (0.950)
  Pallas kernels: 236 us -> 223 us
    pallas_call x1, Pallas kernels: 230 us -> 217 us  [both_half_steps(): pl.pallas_call(functools.partial(kernel, n_fs, n_tp), out_shape=served +...]
where the time goes in v2:
time: 228 us
  Pallas kernels  223 us (98%)
  local copies, waits for them, and re-layouts  3.54 us (2%)
    pallas_call x1, Pallas kernels, both_half_steps(): pl.pallas_call(functools.partial(kernel, n_fs, n_tp), out_shape=served +...  217 us
    pallas_call x1, Pallas kernels, place_results(): pl.pallas_call(place_kernel, out_shape=outs, in_specs=[pl.BlockSpec(memor...  6.22 us

profile of v2, /device:TPU:0, one launch (start us, length us, event | category | flops | bytes accessed | tf_op | source)
XLA Modules:
  0.0 227.6 jit_solution(11842578029069687329)
XLA Ops:
  0.6 0.0 copy-start
  0.6 2.2 copy-done
  2.8 0.0 copy-start.1
  2.8 0.7 copy-done.1
  3.5 0.0 copy-start.2
  3.5 0.7 copy-done.2
  4.2 217.0 %shard_map.144 = (bf16[2,704,2048]{2,1,0:T(8,128)(2,1)S(1)}, bf16[704,2048]{1,0:T(8,128)(2,1)S(1)}, bf16[2,704,2048]{2,1,0:T(8,128)(2,1)S(1)}, bf16[704,2048]{1,0:T(8,128)(2,1)S(1)}, bf16[128,2048]{1,0:T(8,128)(2,1)S(1)}) custom-call(bf16[1024,2048]{1,0:T(8,128)(2,1)S(1)} %bitcast.8, f32[1,256]{1,0:T(1,128)S(1)} %bitcast.9, f32[1,256]{1,0:T(1,128)S(1)} %bitcast.10, ...), custom_call_target="tpu_custom_call" | custom-call | flops 17716740096 | bytes 100663296 | tf_op jit(solution)/shard_map/pallas_call | solution.py:510
  221.2 6.2 %shard_map.145 = (bf16[704,2048]{1,0:T(8,128)(2,1)}, bf16[704,2048]{1,0:T(8,128)(2,1)}, bf16[704,2048]{1,0:T(8,128)(2,1)}, bf16[704,2048]{1,0:T(8,128)(2,1)}, bf...) custom-call(bf16[2,704,2048]{2,1,0:T(8,128)(2,1)S(1)} %get-tuple-element.19.gu_a, ...), custom_call_target="tpu_custom_call" | custom-call | tf_op jit(solution)/shard_map/pallas_call | solution.py:543
Async XLA Ops:
  0.6 2.2 copy-start
  2.8 0.7 copy-start.1
  3.5 0.7 copy-start.2

commit v3 on v2

--- a/solution.py
+++ b/solution.py
@@ -344,7 +344,7 @@
 
 def kernel(n_fs, n_tp, tok, gain_a, gain_b, gate_a, up_a, down_a, gate_b, up_b, down_b,
            gu_out_a, dn_out_a, gu_out_b, dn_out_b, done,
-           staged, staged_dn, gu_a, gu_b, dn_a, dn_b, bounce_a, bounce_b,
+           staged, staged_dn, scale_a, scale_b, gu_a, gu_b, dn_a, dn_b, bounce_a, bounce_b,
            x, part, act, mid, landing, load_sems, *sems):
     n_x = n_tp // CORES
     ring = Ring(n_fs // n_x, n_x)
@@ -360,13 +360,17 @@
     sum_two = Reduce(ring, place, part, landing, rest[2], rest[3])
     spread = Gather(ring, place, x, rest[4], rest[5])
 
-    def load(step, gate, up, down):
-        return [pltpu.make_async_copy(src, dst, load_sems.at[3 * step + i])
-                for i, (src, dst) in enumerate(((gate, staged.at[0]), (up, staged.at[1]), (down, staged_dn)))]
-
-    loads = load(0, gate_a, up_a, down_a)
-    for copy in loads:
-        copy.start()
+    def load(first, *pairs):
+        copies = [pltpu.make_async_copy(src, dst, load_sems.at[first + i]) for i, (src, dst) in enumerate(pairs)]
+        for copy in copies:
+            copy.start()
+        return copies
+
+    own = pl.ds(pl.multiple_of(me_f * share, share), share)
+
+    scales = load(0, (gain_a, scale_a), (gain_b, scale_b))
+    loads = load(2, (gate_a, staged.at[0]), (up_a, staged.at[1]), (down_a, staged_dn))
+    rows_in = load(5, (tok, part), (tok.at[own, :], mid))
 
     barrier = pltpu.get_barrier_semaphore()
 
@@ -392,28 +396,30 @@
     greet(ring.at(place - 1), me_t)
     pl.semaphore_wait(barrier, n_fs + one.n_y + 2 - jnp.where(is_self, 1, 0))
 
+    for copy in scales:
+        copy.wait()
     for kind in range(2):
         loads[kind].wait()
-        fold(staged, gain_a, kind, gu_a)
+        fold(staged, scale_a, kind, gu_a)
         one.start_cross(kind)
         one.near(kind)
     loads[2].wait()
     dn_a[...] = staged_dn[...].astype(dn_a.dtype)
-    loads = load(1, gate_b, up_b, down_b)
-    for copy in loads:
-        copy.start()
+    loads = load(7, (gate_b, staged.at[0]), (up_b, staged.at[1]), (down_b, staged_dn))
+    for copy in rows_in:
+        copy.wait()
 
     @pl.loop(0, n)
     def _(j):
         sign = jnp.where(j % 2 == 0, -1, 1)
         offset = jnp.where(j < 2, j * far, sign * (j // 2))
         f = ring.at(place + offset)
-        rows = tok[pl.ds(pl.multiple_of(f * share, share), share), :].astype(jnp.float32)
+        rows = part[pl.ds(pl.multiple_of(f * share, share), share), :].astype(jnp.float32)
         x[pl.ds(pl.multiple_of(j * share, share), share), :] = normalize(rows)
 
     for kind in range(2):
         loads[kind].wait()
-        fold(staged, gain_b, kind, gu_b)
+        fold(staged, scale_b, kind, gu_b)
         two.start_cross(kind)
         two.near(kind)
     loads[2].wait()
@@ -431,21 +437,20 @@
     def _(j):
         active_rows(x, gu_out_a, act, pl.multiple_of(j * 2 * share, 2 * share), 2 * share)
 
-    two.pass_first(range(n_fs))
     two.start_dn()
     one.pass_dn()
     one.arrive_dn()
-    for s in range(1, far):
-        down_rows(act, dn_out_a, part, 2 * s * share, 2 * share)
-        sum_one.step(s - 1)
-    down_rows(act, dn_out_a, part, 0, 2 * share)
-    for s in range(far - 1, n - 1):
+    for s in range(n - 1):
+        if s < far:
+            down_rows(act, dn_out_a, part, 2 * ((s + 1) % far) * share, 2 * share)
         sum_one.step(s)
-
-    own = pl.ds(pl.multiple_of(me_f * share, share), share)
+        if s == far - 3:
+            two.pass_first(range(n_fs // 2))
+        if s == far - 1:
+            two.pass_first(range(n_fs // 2, n_fs))
 
     def store_middle(cols, total):
-        mid[:, cols] = (tok[own, cols].astype(jnp.float32) + 0.5 * total).astype(mid.dtype)
+        mid[:, cols] = (mid[:, cols].astype(jnp.float32) + 0.5 * total).astype(mid.dtype)
 
     sum_one.last(store_middle)
     x[pl.ds(0, share), :] = normalize(mid[...].astype(jnp.float32))
@@ -510,13 +515,13 @@
     return pl.pallas_call(
         functools.partial(kernel, n_fs, n_tp),
         out_shape=served + served + [jax.ShapeDtypeStruct((share, model), kept)],
-        in_specs=[pl.BlockSpec(memory_space=vmem)] * 3 + [pl.BlockSpec(memory_space=pltpu.HBM)] * 6,
+        in_specs=[pl.BlockSpec(memory_space=pltpu.HBM)] * 9,
         out_specs=[pl.BlockSpec(memory_space=vmem)] * 5,
         scratch_shapes=[
             vmem((2, rows, wide), first[0].dtype), vmem(first[2].shape, first[2].dtype),
-            folded, folded, down, down, bounce, bounce,
+            vmem(gains[0].shape, gains[0].dtype), vmem(gains[1].shape, gains[1].dtype), folded, folded, down, down, bounce, bounce,
             vmem((count, model), kept), vmem((count, model), kept), vmem((count, hidden), kept),
-            vmem((share, model), kept), vmem((2, n_fs - 1, share, model // 2), kept), dma((6,)),
+            vmem((share, model), kept), vmem((2, n_fs - 1, share, model // 2), kept), dma((10,)),
         ] + trade + trade + [hops] * 4 + [spread] * 2,
         compiler_params=pltpu.CompilerParams(
             collective_id=0, has_side_effects=True, vmem_limit_bytes=VMEM_LIMIT
@@ -524,7 +529,7 @@
         cost_estimate=pl.CostEstimate(
             flops=12 * count * model * hidden, bytes_accessed=48 * count * model, transcendentals=0
         ),
-    )(tokens, *gains, *map(stay, first + second))
+    )(*map(stay, (tokens,) + gains + first + second))
 
 
 def place_kernel(gu_a, dn_a, gu_b, dn_b, done, *refs):

time: 228 us -> 223 us (0.978)
  local copies, waits for them, and re-layouts: 3.54 us -> 0 us
    unnamed x6 -> x0, local copies, waits for them, and re-layouts: 3.54 us -> none
where the time goes in v3:
time: 223 us
  Pallas kernels  222 us (100%)
    pallas_call x1, Pallas kernels, both_half_steps(): pl.pallas_call(functools.partial(kernel, n_fs, n_tp), out_shape=served +...  216 us
    pallas_call x1, Pallas kernels, place_results(): pl.pallas_call(place_kernel, out_shape=outs, in_specs=[pl.BlockSpec(memor...  6.22 us

profile of v3, /device:TPU:0, one launch (start us, length us, event | category | flops | bytes accessed | tf_op | source)
XLA Modules:
  0.0 222.7 jit_solution(13883675407587017593)
XLA Ops:
  0.6 215.6 %shard_map.144 = (bf16[2,704,2048]{2,1,0:T(8,128)(2,1)S(1)}, bf16[704,2048]{1,0:T(8,128)(2,1)S(1)}, bf16[2,704,2048]{2,1,0:T(8,128)(2,1)S(1)}, bf16[704,2048]{1,0:T(8,128)(2,1)S(1)}, bf16[128,2048]{1,0:T(8,128)(2,1)S(1)}) custom-call(bf16[1024,2048]{1,0:T(8,128)(2,1)} %bitcast.8, f32[1,256]{1,0:T(1,128)} %bitcast.14, f32[1,256]{1,0:T(1,128)} %bitcast.15, ...), custom_call_target="tpu_custom_call" | custom-call | flops 17716740096 | bytes 100663296 | tf_op jit(solution)/shard_map/pallas_call | solution.py:515
  216.3 6.2 %shard_map.145 = (bf16[704,2048]{1,0:T(8,128)(2,1)}, bf16[704,2048]{1,0:T(8,128)(2,1)}, bf16[704,2048]{1,0:T(8,128)(2,1)}, bf16[704,2048]{1,0:T(8,128)(2,1)}, bf...) custom-call(bf16[2,704,2048]{2,1,0:T(8,128)(2,1)S(1)} %get-tuple-element.19.gu_a, ...), custom_call_target="tpu_custom_call" | custom-call | tf_op jit(solution)/shard_map/pallas_call | solution.py:548

commit v4 on v3

--- a/solution.py
+++ b/solution.py
@@ -97,10 +97,9 @@
         return remote(self.own(kind, i, self.peer(hop)), self.bounce.at[hop - 1, kind, i],
                       self.send_c.at[sem], self.recv_c.at[sem], self.me_f, self.beside(hop))
 
-    def start_cross(self, kind):
+    def start_cross(self, kind, i):
         for hop in range(1, self.n_y):
-            for i in range(self.per):
-                self.cross(hop, kind, i).start()
+            self.cross(hop, kind, i).start()
 
     def deliver(self, src, send, t, kind, i, act):
         f = t * self.per + i
@@ -118,10 +117,18 @@
             def _():
                 pltpu.make_async_copy(src, dst, recv).start()
 
-    def near(self, kind, act=True):
+    def near(self, kind, i, act=True):
+        self.deliver(self.own(kind, i, self.my_y), self.send_n.at[kind * self.per + i], self.me_t,
+                     kind, i, act)
+
+    def fold_and_send(self, staged, gain, kind):
+        done, wide = 0, self.gu.shape[1]
         for i in range(self.per):
-            self.deliver(self.own(kind, i, self.my_y), self.send_n.at[kind * self.per + i], self.me_t,
-                         kind, i, act)
+            stop = min(wide, -(-(i + 1) * self.hidden // LANES) * LANES)
+            fold(staged, gain, kind, self.gu, done, stop)
+            done = stop
+            self.start_cross(kind, i)
+            self.near(kind, i)
 
     def pass_cross(self, act=True):
         for kind in range(2):
@@ -215,7 +222,8 @@
             for hop in range(1, self.n_y):
                 for i in range(self.per):
                     self.cross(hop, kind, i).wait_send()
-            self.near(kind, False)
+            for i in range(self.per):
+                self.near(kind, i, False)
         self.pass_cross(False)
         copies = self.dn_first() + [self.on_dn(hop)[2] for hop in range(1, self.n_y)]
         for step in range(self.n_fs):
@@ -328,18 +336,18 @@
         ).astype(part.dtype)
 
 
-def fold(staged, gain, kind, gu):
-    count = staged.shape[2]
+def fold(staged, gain, kind, gu, start, stop):
+    count = stop - start
 
     def turn(cols, size):
         gu[kind, pl.ds(cols, size), :] = (staged[kind, :, pl.ds(cols, size)].T * gain[...]).astype(gu.dtype)
 
     @pl.loop(0, count // LANES)
     def _(j):
-        turn(pl.multiple_of(j * LANES, LANES), LANES)
+        turn(pl.multiple_of(start + j * LANES, LANES), LANES)
 
     if count % LANES:
-        turn(count - count % LANES, count % LANES)
+        turn(stop - count % LANES, count % LANES)
 
 
 def kernel(n_fs, n_tp, tok, gain_a, gain_b, gate_a, up_a, down_a, gate_b, up_b, down_b,
@@ -370,7 +378,6 @@
 
     scales = load(0, (gain_a, scale_a), (gain_b, scale_b))
     loads = load(2, (gate_a, staged.at[0]), (up_a, staged.at[1]), (down_a, staged_dn))
-    rows_in = load(5, (tok, part), (tok.at[own, :], mid))
 
     barrier = pltpu.get_barrier_semaphore()
 
@@ -400,9 +407,8 @@
         copy.wait()
     for kind in range(2):
         loads[kind].wait()
-        fold(staged, scale_a, kind, gu_a)
-        one.start_cross(kind)
-        one.near(kind)
+        one.fold_and_send(staged, scale_a, kind)
+    rows_in = load(5, (tok, part), (tok.at[own, :], mid))
     loads[2].wait()
     dn_a[...] = staged_dn[...].astype(dn_a.dtype)
     loads = load(7, (gate_b, staged.at[0]), (up_b, staged.at[1]), (down_b, staged_dn))
@@ -419,9 +425,7 @@
 
     for kind in range(2):
         loads[kind].wait()
-        fold(staged, scale_b, kind, gu_b)
-        two.start_cross(kind)
-        two.near(kind)
+        two.fold_and_send(staged, scale_b, kind)
     loads[2].wait()
     dn_b[...] = staged_dn[...].astype(dn_b.dtype)
 
@@ -488,6 +492,7 @@
 
 TRADE_SEMS = 14
 LANES = 128
+PIECES = 2
 VMEM_LIMIT = 32 * 2**20
 
 
@@ -535,7 +540,12 @@
 def place_kernel(gu_a, dn_a, gu_b, dn_b, done, *refs):
     outs, sems = refs[:-1], refs[-1]
     sources = (gu_a.at[0], gu_a.at[1], dn_a, gu_b.at[0], gu_b.at[1], dn_b, done)
-    copies = [pltpu.make_async_copy(src, dst, sems.at[i]) for i, (src, dst) in enumerate(zip(sources, outs))]
+    copies = []
+    for src, dst in zip(sources, outs):
+        rows = src.shape[0] // PIECES
+        for j in range(PIECES):
+            cut = pl.ds(j * rows, rows)
+            copies.append(pltpu.make_async_copy(src.at[cut, :], dst.at[cut, :], sems.at[len(copies)]))
     for copy in copies:
         copy.start()
     for copy in copies:
@@ -550,7 +560,7 @@
         out_shape=outs,
         in_specs=[pl.BlockSpec(memory_space=pltpu.VMEM)] * 5,
         out_specs=[pl.BlockSpec(memory_space=pltpu.HBM)] * 7,
-        scratch_shapes=[pltpu.SemaphoreType.DMA((7,))],
+        scratch_shapes=[pltpu.SemaphoreType.DMA((7 * PIECES,))],
         compiler_params=pltpu.CompilerParams(vmem_limit_bytes=2**20),
     )(gu_a, dn_a, gu_b, dn_b, done)
 

time: 223 us -> 222 us (level)
  no operation moved by 1% of the time
where the time goes in v4:
time: 222 us
  Pallas kernels  221 us (100%)
    pallas_call x1, Pallas kernels, both_half_steps(): pl.pallas_call(functools.partial(kernel, n_fs, n_tp), out_shape=served +...  215 us
    pallas_call x1, Pallas kernels, place_results(): pl.pallas_call(place_kernel, out_shape=outs, in_specs=[pl.BlockSpec(memor...  6.23 us

profile of v4, /device:TPU:0, one launch (start us, length us, event | category | flops | bytes accessed | tf_op | source)
XLA Modules:
  0.0 222.2 jit_solution(3933555411505740045)
XLA Ops:
  0.6 215.1 %shard_map.144 = (bf16[2,704,2048]{2,1,0:T(8,128)(2,1)S(1)}, bf16[704,2048]{1,0:T(8,128)(2,1)S(1)}, bf16[2,704,2048]{2,1,0:T(8,128)(2,1)S(1)}, bf16[704,2048]{1,0:T(8,128)(2,1)S(1)}, bf16[128,2048]{1,0:T(8,128)(2,1)S(1)}) custom-call(bf16[1024,2048]{1,0:T(8,128)(2,1)} %bitcast.8, f32[1,256]{1,0:T(1,128)} %bitcast.14, f32[1,256]{1,0:T(1,128)} %bitcast.15, ...), custom_call_target="tpu_custom_call" | custom-call | flops 17716740096 | bytes 100663296 | tf_op jit(solution)/shard_map/pallas_call | solution.py:520
  215.8 6.2 %shard_map.145 = (bf16[704,2048]{1,0:T(8,128)(2,1)}, bf16[704,2048]{1,0:T(8,128)(2,1)}, bf16[704,2048]{1,0:T(8,128)(2,1)}, bf16[704,2048]{1,0:T(8,128)(2,1)}, bf...) custom-call(bf16[2,704,2048]{2,1,0:T(8,128)(2,1)S(1)} %get-tuple-element.19.gu_a, ...), custom_call_target="tpu_custom_call" | custom-call | tf_op jit(solution)/shard_map/pallas_call | solution.py:558
